TPU v7x, 32 devices: a whole 2x2x4 slice. The times are simulated.
32 devices in a mesh: sp: 16 (over z, y, x), dp: 2 (over core).
Axes of the slice: x: 2, y: 2, z: 4, core: 2. Of those that a mesh axis runs over, the one named last changes fastest.
Arguments:
- tokens: bfloat16 [2048, 2048], P('sp', 'dp'), may hold values from -6 to 6
- cotangent: bfloat16 [2048, 2048], P('sp', 'dp'), may hold values from -6 to 6
- in_weight: bfloat16 [256, 2048], P('sp', 'dp'), may hold values from -0.125 to 0.125
- out_weight: bfloat16 [256, 2048], P('sp', 'dp'), may hold values from -0.375 to 0.375
- decay_rate: float32 [16, 32], P('sp'), may hold values from 0 to 1
- frequency: float32 [16, 32], P('sp'), may hold values from 4 to 40
- step_log: float32 [16], P('sp'), may hold values from -2.6593 to -1.9661
- drive_real: float32 [16, 32, 16], P('sp'), may hold values from -6 to 6
- drive_imag: float32 [16, 32, 16], P('sp'), may hold values from -6 to 6
- readout_real_part: float32 [16, 16, 32], P('sp'), may hold values from -0.75 to 0.75
- readout_imaginary: float32 [16, 16, 32], P('sp'), may hold values from -0.75 to 0.75
- skip_gain: float32 [16, 16], P('sp'), may hold values from -4 to 4
Outputs:
- grad_tokens: bfloat16 [2048, 2048], P('sp', 'dp')
- grad_in_weight: float32 [256, 2048], P('sp', 'dp')
- grad_out_weight: float32 [256, 2048], P('sp', 'dp')
All inputs are finite; a program needn't handle non-finite values.
Results may differ from a plain program's by a relative error of at most 0.02.
Values may be sent and summed in bfloat16 or wider, within the bound.
A program may use at most 64 MiB of HBM per device.

v0:
```python
import jax
import jax.numpy as jnp
from jax import lax
from jax.sharding import PartitionSpec as P

finest_precision = lax.Precision.HIGHEST


def combine(earlier, later):
    first_real, first_imag, first_sum_real, first_sum_imag = earlier
    next_real, next_imag, next_sum_real, next_sum_imag = later
    return (
        first_real * next_real - first_imag * next_imag,
        first_real * next_imag + first_imag * next_real,
        next_real * first_sum_real - next_imag * first_sum_imag + next_sum_real,
        next_real * first_sum_imag + next_imag * first_sum_real + next_sum_imag,
    )


def discretize(decay_rate, frequency, step_log, drive_real, drive_imag):
    step_size = jnp.exp(step_log)[..., None]
    magnitude = jnp.exp(-decay_rate * step_size)
    angle = frequency * step_size
    decay_real = magnitude * jnp.cos(angle)
    decay_imag = magnitude * jnp.sin(angle)
    modulus = decay_rate * decay_rate + frequency * frequency
    hold_real = (-decay_rate * (decay_real - 1.0) + frequency * decay_imag) / modulus
    hold_imag = (-frequency * (decay_real - 1.0) - decay_rate * decay_imag) / modulus
    input_real = hold_real[..., None] * drive_real - hold_imag[..., None] * drive_imag
    input_imag = hold_real[..., None] * drive_imag + hold_imag[..., None] * drive_real
    return (decay_real, decay_imag, input_real, input_imag)


def mechanism(head_drive, head_back, params):
    (
        decay_rate,
        frequency,
        step_log,
        drive_real,
        drive_imag,
        readout_real_part,
        readout_imaginary,
        skip_gain,
    ) = params
    group_count, states = decay_rate.shape
    own_width, length = head_drive.shape
    per_group = own_width // group_count
    block_len = min(512, length)
    blocks_total = length // block_len
    decay_real, decay_imag, input_real, input_imag = discretize(
        decay_rate, frequency, step_log, drive_real, drive_imag
    )
    factor_real = jnp.broadcast_to(decay_real[:, :, None], (group_count, states, block_len))
    factor_imag = jnp.broadcast_to(decay_imag[:, :, None], (group_count, states, block_len))

    def to_blocks(matrix):
        shaped = matrix.astype(jnp.float32).reshape(group_count, per_group, blocks_total, block_len)
        return jnp.moveaxis(shaped, 2, 0)

    def forward(carried, drive_block):
        state_real, state_imag = carried
        push_real = jnp.einsum("gpc,gck->gpk", input_real, drive_block, precision=finest_precision)
        push_imag = jnp.einsum("gpc,gck->gpk", input_imag, drive_block, precision=finest_precision)
        push_real = push_real.at[:, :, 0].add(decay_real * state_real - decay_imag * state_imag)
        push_imag = push_imag.at[:, :, 0].add(decay_real * state_imag + decay_imag * state_real)
        _, _, running_real_part, running_imaginary = lax.associative_scan(
            combine, (factor_real, factor_imag, push_real, push_imag), axis=2
        )
        mixed_rows = (
            jnp.einsum(
                "mow,mwn->mon", readout_real_part, running_real_part, precision=finest_precision
            )
            - jnp.einsum(
                "mow,mwn->mon", readout_imaginary, running_imaginary, precision=finest_precision
            )
            + skip_gain[:, :, None] * drive_block
        )
        return ((running_real_part[:, :, -1], running_imaginary[:, :, -1]), mixed_rows)

    empty_state = jnp.zeros((group_count, states), jnp.float32)
    _, mixed_blocks = lax.scan(forward, (empty_state, empty_state), to_blocks(head_drive))

    def backward(carried, inputs):
        adjoint_real, adjoint_imag = carried
        mixed_rows, back_block = inputs
        gated, pullback = jax.vjp(jax.nn.gelu, mixed_rows)
        (interior_gradient,) = pullback(back_block)
        pulled_real_part = jnp.einsum(
            "woy,wom->wym", readout_real_part, interior_gradient, precision=finest_precision
        )[:, :, ::-1]
        pulled_imaginary = -jnp.einsum(
            "woy,wom->wym", readout_imaginary, interior_gradient, precision=finest_precision
        )[:, :, ::-1]
        pulled_real_part = pulled_real_part.at[:, :, 0].add(
            decay_real * adjoint_real + decay_imag * adjoint_imag
        )
        pulled_imaginary = pulled_imaginary.at[:, :, 0].add(
            decay_real * adjoint_imag - decay_imag * adjoint_real
        )
        _, _, running_real_part, running_imaginary = lax.associative_scan(
            combine, (factor_real, -factor_imag, pulled_real_part, pulled_imaginary), axis=2
        )
        running_real_part = running_real_part[:, :, ::-1]
        running_imaginary = running_imaginary[:, :, ::-1]
        grad_block = (
            jnp.einsum("gpc,gpk->gck", input_real, running_real_part, precision=finest_precision)
            + jnp.einsum("gpc,gpk->gck", input_imag, running_imaginary, precision=finest_precision)
            + skip_gain[:, :, None] * interior_gradient
        )
        return (
            (running_real_part[:, :, 0], running_imaginary[:, :, 0]),
            (grad_block.astype(jnp.bfloat16), gated.astype(jnp.bfloat16)),
        )

    _, (grad_blocks, gated_blocks) = lax.scan(
        backward, (empty_state, empty_state), (mixed_blocks, to_blocks(head_back)), reverse=True
    )

    def from_blocks(stacked):
        return jnp.moveaxis(stacked, 0, 2).reshape(own_width, length)

    return (from_blocks(grad_blocks), from_blocks(gated_blocks))


def on_device(
    tokens,
    cotangent,
    in_weight,
    out_weight,
    decay_rate,
    frequency,
    step_log,
    drive_real,
    drive_imag,
    readout_real_part,
    readout_imaginary,
    skip_gain,
):
    full_in, full_out = (
        lax.all_gather(in_weight, "sp", axis=0, tiled=True),
        lax.all_gather(out_weight, "sp", axis=0, tiled=True),
    )
    part_drive = jnp.einsum(
        "cd,td->ct", full_in, tokens, preferred_element_type=jnp.float32
    ).astype(jnp.bfloat16)
    part_back = jnp.einsum(
        "cd,td->ct", full_out, cotangent, preferred_element_type=jnp.float32
    ).astype(jnp.bfloat16)
    channels = part_drive.shape[0]
    rows_here = tokens.shape[0]
    seq_devices = lax.axis_size("sp")
    own_width = channels // seq_devices
    params = (
        decay_rate,
        frequency,
        step_log,
        drive_real,
        drive_imag,
        readout_real_part,
        readout_imaginary,
        skip_gain,
    )
    row_groups = lax.axis_size("dp")
    portion = rows_here // row_groups
    own_slot = lax.axis_index("dp") * portion
    drive_share, back_share = (
        lax.psum_scatter(part_drive, "dp", scatter_dimension=1, tiled=True).astype(jnp.float32),
        lax.psum_scatter(part_back, "dp", scatter_dimension=1, tiled=True).astype(jnp.float32),
    )
    drive_slice = drive_share.astype(jnp.bfloat16)[:, None, :]
    back_slice = back_share.astype(jnp.bfloat16)[:, None, :]
    drive_parts, back_parts = (
        lax.all_to_all(drive_slice, "sp", split_axis=0, concat_axis=1, tiled=True),
        lax.all_to_all(back_slice, "sp", split_axis=0, concat_axis=1, tiled=True),
    )
    drive_joined, back_joined = (
        lax.all_gather(drive_parts, "dp", axis=2, tiled=True),
        lax.all_gather(back_parts, "dp", axis=2, tiled=True),
    )
    head_grad, head_gated = mechanism(
        drive_joined.reshape(own_width, seq_devices * rows_here),
        back_joined.reshape(own_width, seq_devices * rows_here),
        params,
    )
    grad_slice = lax.dynamic_slice_in_dim(
        head_grad.reshape(own_width, seq_devices, rows_here), own_slot, portion, 2
    )
    gated_slice = lax.dynamic_slice_in_dim(
        head_gated.reshape(own_width, seq_devices, rows_here), own_slot, portion, 2
    )
    grad_parts, gated_parts = (
        lax.all_to_all(grad_slice, "sp", split_axis=1, concat_axis=0, tiled=True),
        lax.all_to_all(gated_slice, "sp", split_axis=1, concat_axis=0, tiled=True),
    )
    grad_joined, gated_joined = (
        lax.all_gather(grad_parts, "dp", axis=2, tiled=True),
        lax.all_gather(gated_parts, "dp", axis=2, tiled=True),
    )
    grad_cols = grad_joined.reshape(channels, rows_here)
    gated_cols = gated_joined.reshape(channels, rows_here)
    grad_tokens = jnp.einsum(
        "ct,cd->td", grad_cols, full_in, preferred_element_type=jnp.float32
    ).astype(jnp.bfloat16)
    grad_scale = (rows_here * seq_devices) ** (-0.5)
    picked = grad_cols
    grad_in_weight = lax.psum_scatter(
        jnp.einsum("ct,td->cd", picked, tokens, preferred_element_type=jnp.float32) * grad_scale,
        "sp",
        scatter_dimension=0,
        tiled=True,
    )
    picked = gated_cols
    grad_out_weight = lax.psum_scatter(
        jnp.einsum("ct,td->cd", picked, cotangent, preferred_element_type=jnp.float32) * grad_scale,
        "sp",
        scatter_dimension=0,
        tiled=True,
    )
    return (grad_tokens, grad_in_weight, grad_out_weight)


def solution(mesh):
    return jax.shard_map(
        on_device,
        mesh=mesh,
        in_specs=(
            P("sp", "dp"),
            P("sp", "dp"),
            P("sp", "dp"),
            P("sp", "dp"),
            P("sp", None),
            P("sp", None),
            P("sp"),
            P("sp", None, None),
            P("sp", None, None),
            P("sp", None, None),
            P("sp", None, None),
            P("sp", None),
        ),
        out_specs=(P("sp", "dp"), P("sp", "dp"), P("sp", "dp")),
        check_vma=False,
    )
```

profile of v0, /device:TPU:0, one launch (start us, length us, event | category | flops | bytes accessed | tf_op | source)
XLA Modules:
  0.0 653.4 jit_solution(1180258322243700626)
XLA Ops:
  7.2 45.7 %all_gather.20 = bf16[256,1024]{1,0:T(8,128)(2,1)S(1)} all-gather(bf16[16,1024]{1,0:T(8,128)(2,1)} %param.26), channel_id=1, replica_groups=mesh['sp'=16,'dp'=2] {'sp'}, dimensions={0}, use_global_device_ids=true | all-gather | bytes 557056 | tf_op jit(solution)/shard_map/all_gather | solution.py:140
  54.6 38.5 %all_gather.18 = bf16[256,1024]{1,0:T(8,128)(2,1)S(1)} all-gather(bf16[16,1024]{1,0:T(8,128)(2,1)S(1)} %copy-done.4), channel_id=1, replica_groups=mesh['sp'=16,'dp'=2] {'sp'}, dimensions={0}, use_global_device_ids=true | all-gather | bytes 557056 | tf_op jit(solution)/shard_map/all_gather | solution.py:141
  96.9 1.4 reduce.23
  99.1 3.5 all-to-all-start.1
  103.0 1.4 reduce.22
  105.2 4.8 all-to-all-done.1
  110.0 3.5 all-to-all-start
  114.0 2.2 all-gather.1
  118.6 164.4 %while.40 = (s32[]{:T(128)}, f32[1,32]{1,0:T(1,128)S(1)}, f32[1,32]{1,0:T(1,128)S(1)}, f32[4,1,16,512]{3,2,1,0:T(8,128)S(1)}, f32[4,1,16,512]{3,0,2,1:T(4,128)S(...) while((s32[]{:T(128)}, f32[1,32]{1,0:T(1,128)S(1)}, ...), condition=%wide.region_2.3_spmd, body=%wide.region_1.0_spmd.sunk | while | flops 12997378 | bytes 4572589 | solution.py:81
  120.7 1.1 slice.2926
  123.1 1.1 slice.2925
  124.2 1.1 slice.2922
  125.4 1.1 slice.2924
  161.7 1.1 slice.2926
  164.1 1.1 slice.2925
  165.3 1.1 slice.2922
  166.4 1.1 slice.2924
  202.8 1.1 slice.2926
  205.2 1.1 slice.2925
  206.3 1.1 slice.2922
  207.5 1.1 slice.2924
  243.8 1.1 slice.2926
  246.3 1.1 slice.2925
  247.4 1.1 slice.2922
  248.5 1.1 slice.2924
  283.4 2.2 all-gather
  287.3 188.4 %while.41 = (s32[]{:T(128)}, f32[1,32]{1,0:T(1,128)S(1)}, f32[1,32]{1,0:T(1,128)S(1)}, bf16[4,1,16,512]{3,2,1,0:T(8,128)(2,1)S(1)}, bf16[4,1,16,512]{3,2,1,0:T(8...) while((s32[]{:T(128)}, f32[1,32]{1,0:T(1,128)S(1)}, ...), condition=%wide.region_5.6_spmd, body=%wide.region_4.0_spmd.sunk | while | flops 13562627 | bytes 5699549 | solution.py:115
  307.7 1.1 slice.3051
  310.2 1.1 slice.3050
  311.3 1.1 slice.3047
  312.5 1.1 slice.3049
  344.3 1.1 pad.1013
  350.4 1.1 slice.3051
  352.8 1.1 slice.3050
  354.0 1.1 slice.3047
  387.0 1.1 pad.1013
  395.5 1.1 slice.3050
  429.6 1.1 pad.1013
  438.2 1.1 slice.3050
  472.3 1.1 pad.1013
  476.2 14.1 %all_to_all.72 = bf16[16,2,512]{2,1,0:T(2,128)(2,1)S(1)} all-to-all(bf16[16,2,512]{2,1,0:T(2,128)(2,1)S(1)} %reshape.604), channel_id=1, replica_groups=mesh['sp'=16,'dp'=2] {'sp'}, dimensions={0} | all-to-all | bytes 65536 | tf_op jit(solution)/shard_map/all_to_all | solution.py:193
  490.4 1.9 all_gather.23
  492.3 1.3 convolution_multiply_fusion
  493.8 10.1 %all_to_all.73 = bf16[16,2,512]{2,1,0:T(2,128)(2,1)S(1)} all-to-all(bf16[16,2,512]{2,1,0:T(2,128)(2,1)S(1)} %reshape.602), channel_id=1, replica_groups=mesh['sp'=16,'dp'=2] {'sp'}, dimensions={0} | all-to-all | bytes 65536 | tf_op jit(solution)/shard_map/all_to_all | solution.py:192
  504.1 1.9 all_gather.22
  506.0 1.3 convolution_multiply_fusion.1
  508.2 60.7 %reduce-scatter.11.cloned.1.call-done = f32[16,1024]{1,0:T(8,128)} async-done(((f32[256,1024]{1,0:T(8,128)}), f32[16,1024]{1,0:T(8,128)}) %reduce-scatter.11.cloned.1.call-update) | async-done | bytes 65552 | tf_op jit(solution)/shard_map/reduce_scatter | solution.py:213
  568.9 77.7 %reduce-scatter.9.cloned.1.call-done = f32[16,1024]{1,0:T(8,128)} async-done(((f32[256,1024]{1,0:T(8,128)}), f32[16,1024]{1,0:T(8,128)}) %reduce-scatter.9.cloned.1.call-update) | async-done | bytes 65552 | tf_op jit(solution)/shard_map/reduce_scatter | solution.py:206
  (1484 shorter events, 307.8 us)
Async XLA Ops:
  7.2 86.0 %copy-start = (bf16[128,1024]{1,0:T(8,128)(2,1)S(1)}, bf16[128,1024]{1,0:T(8,128)(2,1)}, u32[]{:S(2)}) copy-start(bf16[128,1024]{1,0:T(8,128)(2,1)} %param.25) | copy-start | bytes 786436
  7.2 45.7 %copy-start.1 = (bf16[128,1024]{1,0:T(8,128)(2,1)S(1)}, bf16[128,1024]{1,0:T(8,128)(2,1)}, u32[]{:S(2)}) copy-start(bf16[128,1024]{1,0:T(8,128)(2,1)} %param.24) | copy-start | bytes 786436
  7.2 89.1 %reduce-scatter.7.cloned.1.call-start = ((), (), s32[]{:S(2)}) async-start(), calls=%async_computation.9 | async-start | bytes 98304 | tf_op jit(solution)/shard_map/reduce_scatter | solution.py:167
  53.9 0.8 copy-start.4
  53.9 49.1 %reduce-scatter.5.cloned.1.call-start = ((), (), s32[]{:S(2)}) async-start(), calls=%async_computation.8 | async-start | bytes 98304 | tf_op jit(solution)/shard_map/reduce_scatter | solution.py:168
  94.8 0.7 copy-start.8
  94.9 0.7 copy-start.9
  95.6 0.7 copy-start.6
  95.6 0.7 copy-start.7
  99.1 10.9 %all-to-all-start.1 = ((bf16[16,2,512]{2,1,0:T(2,128)(2,1)}), bf16[16,2,512]{2,1,0:T(2,128)(2,1)S(1)}, u32[]{:S(2)}, u32[]{:S(2)}) async-start(bf16[16,2,512]{2,1,0:T(2,128)(2,1)} %reshape.600), calls=%async_computation.3 | async-start | bytes 65536 | tf_op jit(solution)/shard_map/all_to_all | solution.py:173
  110.0 173.0 %all-to-all-start = ((bf16[16,2,512]{2,1,0:T(2,128)(2,1)}), bf16[16,2,512]{2,1,0:T(2,128)(2,1)S(1)}, u32[]{:S(2)}, u32[]{:S(2)}) async-start(bf16[16,2,512]{2,1,0:T(2,128)(2,1)} %reshape.598), calls=%async_computation.1 | async-start | bytes 65536 | tf_op jit(solution)/shard_map/all_to_all | solution.py:174
  113.5 455.4 %reduce-scatter.11.cloned.1.call-start = ((), (), s32[]{:S(2)}) async-start(), calls=%async_computation.11 | async-start | bytes 1114112 | tf_op jit(solution)/shard_map/reduce_scatter | solution.py:213
  117.8 0.7 copy-start.2
  117.8 0.7 copy-start.3
  117.9 0.7 copy-start.5
  493.6 153.0 %reduce-scatter.9.cloned.1.call-start = ((), (), s32[]{:S(2)}) async-start(), calls=%async_computation.10 | async-start | bytes 1114112 | tf_op jit(solution)/shard_map/reduce_scatter | solution.py:206
Sparse Core Ops, SparseCore 0:
  54.0 3.3 reduce-scatter.6
  94.3 5.1 reduce-scatter.4
  493.7 75.1 reduce-scatter.10
  571.6 75.0 reduce-scatter.8
where the time goes:
time: 657 us; the launch traced here: 653 us
  local copies, waits for them, and re-layouts  313 us (48%)
  waiting for transfers between devices  143 us (22%)
  blocking collectives  117 us (18%)
  loops' own time  25.5 us (4%)
  other arithmetic  20.8 us (3%)
  between operations  14.9 us (2%)
  matrix products  11.7 us (2%)
  starting transfers between devices  7.16 us (1%)
    slice x328, local copies, waits for them, and re-layouts, forward(): lax.associative_scan(combine, (factor_real, factor_imag, push_real, push_...  106 us
    slice x327, local copies, waits for them, and re-layouts, backward(): lax.associative_scan(combine, (factor_real, -factor_imag, pulled_real_par...  106 us
    reduce_scatter x1, waiting for transfers between devices, on_device(): lax.psum_scatter(jnp.einsum('ct,td->cd', picked, tokens, preferred_elemen...  77.7 us
    reduce_scatter x1, waiting for transfers between devices, on_device(): lax.psum_scatter(jnp.einsum('ct,td->cd', picked, cotangent, preferred_ele...  60.7 us
    all_gather x1, blocking collectives, on_device(): lax.all_gather(in_weight, 'sp', axis=0, tiled=True)  45.7 us
    pad x128, local copies, waits for them, and re-layouts, backward(): lax.associative_scan(combine, (factor_real, -factor_imag, pulled_real_par...  41.8 us
    pad x128, local copies, waits for them, and re-layouts, forward(): lax.associative_scan(combine, (factor_real, factor_imag, push_real, push_...  41.8 us
    all_gather x1, blocking collectives, on_device(): lax.all_gather(out_weight, 'sp', axis=0, tiled=True)  38.5 us
  transfers between devices with their start and end apart: 6, of which 3 were waited for; matrix products, arithmetic and copies ran while one was open for 26% of the time, Pallas kernels for 0%

commit v1 on v0

--- a/solution.py
+++ b/solution.py
@@ -4,6 +4,13 @@
 from jax.sharding import PartitionSpec as P
 
 finest_precision = lax.Precision.HIGHEST
+
+
+def swapped_in(x, axis, dim):
+    count = lax.axis_size(axis)
+    parts = jnp.stack([x for _ in range(count)])
+    parts = lax.all_to_all(parts, axis, split_axis=0, concat_axis=0)
+    return jnp.concatenate(parts, axis=dim)
 
 
 def combine(earlier, later):
@@ -137,7 +144,7 @@
     skip_gain,
 ):
     full_in, full_out = (
-        lax.all_gather(in_weight, "sp", axis=0, tiled=True),
+        swapped_in(in_weight, "sp", 0),
         lax.all_gather(out_weight, "sp", axis=0, tiled=True),
     )
     part_drive = jnp.einsum(

time: 657 us -> 644 us (0.980)
  blocking collectives: 117 us -> 74.2 us
  waiting for transfers between devices: 143 us -> 158 us
  starting transfers between devices: 7.16 us -> 22.1 us
    all_gather x1 -> x0, blocking collectives: 45.7 us -> none  [on_device(): lax.all_gather(in_weight, 'sp', axis=0, tiled=True)]
    reduce_scatter x1, waiting for transfers between devices: 0.01 us -> 11.4 us  [on_device(): lax.psum_scatter(part_drive, 'dp', scatter_dimension=1, tiled=True)]
    all_to_all x0 -> x1, starting transfers between devices: none -> 8.47 us  [swapped_in(): parts = lax.all_to_all(parts, axis, split_axis=0, concat_axis=0)]
    all_gather x1, blocking collectives: 38.5 us -> 45.8 us  [on_device(): lax.all_gather(out_weight, 'sp', axis=0, tiled=True)]
  transfers between devices with their start and end apart: 6 -> 7, of which waited for: 3 -> 5; matrix products, arithmetic and copies ran while one was open for 26% -> 2% of each run, Pallas kernels for 0% -> 0%
where the time goes in v1:
time: 644 us; the launch traced here: 640 us
  local copies, waits for them, and re-layouts  313 us (49%)
  waiting for transfers between devices  158 us (25%)
  blocking collectives  74.2 us (12%)
  loops' own time  25.5 us (4%)
  starting transfers between devices  22.1 us (3%)
  other arithmetic  20.9 us (3%)
  between operations  15 us (2%)
  matrix products  11.8 us (2%)
    slice x328, local copies, waits for them, and re-layouts, forward(): lax.associative_scan(combine, (factor_real, factor_imag, push_real, push_...  106 us
    slice x327, local copies, waits for them, and re-layouts, backward(): lax.associative_scan(combine, (factor_real, -factor_imag, pulled_real_par...  106 us
    reduce_scatter x1, waiting for transfers between devices, on_device(): lax.psum_scatter(jnp.einsum('ct,td->cd', picked, tokens, preferred_elemen...  77.7 us
    reduce_scatter x1, waiting for transfers between devices, on_device(): lax.psum_scatter(jnp.einsum('ct,td->cd', picked, cotangent, preferred_ele...  60.7 us
    all_gather x1, blocking collectives, on_device(): lax.all_gather(out_weight, 'sp', axis=0, tiled=True)  45.8 us
    pad x128, local copies, waits for them, and re-layouts, backward(): lax.associative_scan(combine, (factor_real, -factor_imag, pulled_real_par...  41.8 us
    pad x128, local copies, waits for them, and re-layouts, forward(): lax.associative_scan(combine, (factor_real, factor_imag, push_real, push_...  41.8 us
    another operation x1, loops' own time, mechanism(): lax.scan(backward, (empty_state, empty_state), (mixed_blocks, to_blocks(h...  21.6 us
  transfers between devices with their start and end apart: 7, of which 5 were waited for; matrix products, arithmetic and copies ran while one was open for 2% of the time, Pallas kernels for 0%

profile of v1, /device:TPU:0, one launch (start us, length us, event | category | flops | bytes accessed | tf_op | source)
XLA Modules:
  0.0 640.4 jit_solution(13633234733847197750)
XLA Ops:
  7.2 1.7 stack.2
  8.8 8.5 %all-to-all-start.1 = ((bf16[16,16,1024]{2,1,0:T(8,128)(2,1)}), bf16[16,16,1024]{2,1,0:T(8,128)(2,1)S(1)}, u32[]{:S(2)}, u32[]{:S(2)}) async-start(bf16[16,16,1024]{2,1,0:T(8,128)(2,1)} %stack.2), calls=%async_computation.2 | async-start | bytes 1048576 | tf_op jit(solution)/shard_map/all_to_all | solution.py:12
  17.4 45.8 %all_gather.15 = bf16[256,1024]{1,0:T(8,128)(2,1)S(1)} all-gather(bf16[16,1024]{1,0:T(8,128)(2,1)S(1)} %copy-done.4), channel_id=1, replica_groups=mesh['sp'=16,'dp'=2] {'sp'}, dimensions={0}, use_global_device_ids=true | all-gather | bytes 557056 | tf_op jit(solution)/shard_map/all_gather | solution.py:148
  65.1 4.2 reduce-scatter.5.cloned.1.call-done
  69.8 1.4 reduce.22
  72.0 6.7 %all-to-all-start = ((bf16[16,2,512]{2,1,0:T(2,128)(2,1)}), bf16[16,2,512]{2,1,0:T(2,128)(2,1)S(1)}, u32[]{:S(2)}, u32[]{:S(2)}) async-start(bf16[16,2,512]{2,1,0:T(2,128)(2,1)} %reshape.604), calls=%async_computation.1 | async-start | bytes 65536 | tf_op jit(solution)/shard_map/all_to_all | solution.py:181
  79.8 11.4 %reduce-scatter.7.cloned.1.call-done = bf16[256,64]{0,1:T(8,128)(2,1)} async-done(((bf16[256,128]{0,1:T(8,128)(2,1)}), bf16[256,64]{0,1:T(8,128)(2,1)}) %reduce-scatter.7.cloned.1.call-update) | async-done | bytes 32784 | tf_op jit(solution)/shard_map/reduce_scatter | solution.py:174
  91.2 1.4 reduce.23
  93.5 6.7 %all-to-all-start.2 = ((bf16[16,2,512]{2,1,0:T(2,128)(2,1)}), bf16[16,2,512]{2,1,0:T(2,128)(2,1)S(1)}, u32[]{:S(2)}, u32[]{:S(2)}) async-start(bf16[16,2,512]{2,1,0:T(2,128)(2,1)} %reshape.606), calls=%async_computation.4 | async-start | bytes 65536 | tf_op jit(solution)/shard_map/all_to_all | solution.py:180
  101.0 2.2 all-gather
  103.7 3.9 all-to-all-done.2
  108.0 2.2 all-gather.1
  112.7 164.4 %while.40 = (s32[]{:T(128)}, f32[1,32]{1,0:T(1,128)S(1)}, f32[1,32]{1,0:T(1,128)S(1)}, f32[4,1,16,512]{3,2,1,0:T(8,128)S(1)}, f32[4,1,16,512]{3,0,2,1:T(4,128)S(...) while((s32[]{:T(128)}, f32[1,32]{1,0:T(1,128)S(1)}, ...), condition=%wide.region_2.3_spmd, body=%wide.region_1.0_spmd.sunk | while | flops 12997378 | bytes 4572589 | solution.py:88
  114.7 1.1 slice.2926
  117.1 1.1 slice.2925
  118.3 1.1 slice.2922
  119.4 1.1 slice.2924
  155.8 1.1 slice.2926
  158.2 1.1 slice.2925
  159.3 1.1 slice.2922
  160.5 1.1 slice.2924
  196.8 1.1 slice.2926
  199.2 1.1 slice.2925
  201.5 1.1 slice.2924
  240.3 1.1 slice.2925
  242.6 1.1 slice.2924
  278.3 188.4 %while.41 = (s32[]{:T(128)}, f32[1,32]{1,0:T(1,128)S(1)}, f32[1,32]{1,0:T(1,128)S(1)}, bf16[4,1,16,512]{3,2,1,0:T(8,128)(2,1)S(1)}, bf16[4,1,16,512]{3,2,1,0:T(8...) while((s32[]{:T(128)}, f32[1,32]{1,0:T(1,128)S(1)}, ...), condition=%wide.region_5.6_spmd, body=%wide.region_4.0_spmd.sunk | while | flops 13562627 | bytes 5699549 | solution.py:122
  301.2 1.1 slice.3050
  335.3 1.1 pad.1013
  343.8 1.1 slice.3050
  346.1 1.1 slice.3049
  377.9 1.1 pad.1013
  386.5 1.1 slice.3050
  387.6 1.1 slice.3047
  388.8 1.1 slice.3049
  420.6 1.1 pad.1013
  426.7 1.1 slice.3051
  429.2 1.1 slice.3050
  430.3 1.1 slice.3047
  463.3 1.1 pad.1013
  467.1 10.2 %all_to_all.77 = bf16[16,2,512]{2,1,0:T(2,128)(2,1)S(1)} all-to-all(bf16[16,2,512]{2,1,0:T(2,128)(2,1)S(1)} %reshape.610), channel_id=1, replica_groups=mesh['sp'=16,'dp'=2] {'sp'}, dimensions={0} | all-to-all | bytes 65536 | tf_op jit(solution)/shard_map/all_to_all | solution.py:200
  477.5 1.9 all_gather.19
  479.4 1.3 convolution_multiply_fusion
  480.9 10.1 %all_to_all.78 = bf16[16,2,512]{2,1,0:T(2,128)(2,1)S(1)} all-to-all(bf16[16,2,512]{2,1,0:T(2,128)(2,1)S(1)} %reshape.608), channel_id=1, replica_groups=mesh['sp'=16,'dp'=2] {'sp'}, dimensions={0} | all-to-all | bytes 65536 | tf_op jit(solution)/shard_map/all_to_all | solution.py:199
  491.2 1.9 all_gather.18
  493.1 1.3 convolution_multiply_fusion.1
  495.3 60.7 %reduce-scatter.11.cloned.1.call-done = f32[16,1024]{1,0:T(8,128)} async-done(((f32[256,1024]{1,0:T(8,128)}), f32[16,1024]{1,0:T(8,128)}) %reduce-scatter.11.cloned.1.call-update) | async-done | bytes 65552 | tf_op jit(solution)/shard_map/reduce_scatter | solution.py:220
  556.0 77.7 %reduce-scatter.9.cloned.1.call-done = f32[16,1024]{1,0:T(8,128)} async-done(((f32[256,1024]{1,0:T(8,128)}), f32[16,1024]{1,0:T(8,128)}) %reduce-scatter.9.cloned.1.call-update) | async-done | bytes 65552 | tf_op jit(solution)/shard_map/reduce_scatter | solution.py:213
  (1486 shorter events, 309.2 us)
Async XLA Ops:
  7.2 56.0 %copy-start = (bf16[128,1024]{1,0:T(8,128)(2,1)S(1)}, bf16[128,1024]{1,0:T(8,128)(2,1)}, u32[]{:S(2)}) copy-start(bf16[128,1024]{1,0:T(8,128)(2,1)} %param.25) | copy-start | bytes 786436
  8.8 8.5 %copy-start.4 = (bf16[16,1024]{1,0:T(8,128)(2,1)S(1)}, bf16[16,1024]{1,0:T(8,128)(2,1)}, u32[]{:S(2)}) copy-start(bf16[16,1024]{1,0:T(8,128)(2,1)} %param.27) | copy-start | bytes 98308
  8.8 63.2 %all-to-all-start.1 = ((bf16[16,16,1024]{2,1,0:T(8,128)(2,1)}), bf16[16,16,1024]{2,1,0:T(8,128)(2,1)S(1)}, u32[]{:S(2)}, u32[]{:S(2)}) async-start(bf16[16,16,1024]{2,1,0:T(8,128)(2,1)} %stack.2), calls=%async_computation.2 | async-start | bytes 1048576 | tf_op jit(solution)/shard_map/all_to_all | solution.py:12
  17.3 51.9 %reduce-scatter.5.cloned.1.call-start = ((), (), s32[]{:S(2)}) async-start(), calls=%async_computation.9 | async-start | bytes 98304 | tf_op jit(solution)/shard_map/reduce_scatter | solution.py:175
  63.2 1.7 copy-start.8
  63.2 1.7 copy-start.9
  63.2 1.8 copy-start.6
  63.2 1.8 copy-start.7
  64.2 14.7 %copy-start.1 = (bf16[128,1024]{1,0:T(8,128)(2,1)S(1)}, bf16[128,1024]{1,0:T(8,128)(2,1)}, u32[]{:S(2)}) copy-start(bf16[128,1024]{1,0:T(8,128)(2,1)} %param.24) | copy-start | bytes 786436
  72.0 21.5 %all-to-all-start = ((bf16[16,2,512]{2,1,0:T(2,128)(2,1)}), bf16[16,2,512]{2,1,0:T(2,128)(2,1)S(1)}, u32[]{:S(2)}, u32[]{:S(2)}) async-start(bf16[16,2,512]{2,1,0:T(2,128)(2,1)} %reshape.604), calls=%async_computation.1 | async-start | bytes 65536 | tf_op jit(solution)/shard_map/all_to_all | solution.py:181
  78.8 12.4 %reduce-scatter.7.cloned.1.call-start = ((), (), s32[]{:S(2)}) async-start(), calls=%async_computation.10 | async-start | bytes 98304 | tf_op jit(solution)/shard_map/reduce_scatter | solution.py:174
  93.5 14.1 %all-to-all-start.2 = ((bf16[16,2,512]{2,1,0:T(2,128)(2,1)}), bf16[16,2,512]{2,1,0:T(2,128)(2,1)S(1)}, u32[]{:S(2)}, u32[]{:S(2)}) async-start(bf16[16,2,512]{2,1,0:T(2,128)(2,1)} %reshape.606), calls=%async_computation.4 | async-start | bytes 65536 | tf_op jit(solution)/shard_map/all_to_all | solution.py:180
  100.2 455.8 %reduce-scatter.11.cloned.1.call-start = ((), (), s32[]{:S(2)}) async-start(), calls=%async_computation.12 | async-start | bytes 1114112 | tf_op jit(solution)/shard_map/reduce_scatter | solution.py:220
  111.9 0.7 copy-start.2
  111.9 0.7 copy-start.3
  112.0 0.7 copy-start.5
  480.7 152.9 %reduce-scatter.9.cloned.1.call-start = ((), (), s32[]{:S(2)}) async-start(), calls=%async_computation.11 | async-start | bytes 1114112 | tf_op jit(solution)/shard_map/reduce_scatter | solution.py:213
Sparse Core Ops, SparseCore 0:
  64.3 4.8 reduce-scatter.4
  82.3 8.8 reduce-scatter.6
  480.8 75.1 reduce-scatter.10
  558.7 74.9 reduce-scatter.8
